TPU v7x, 512 devices: a whole 4x4x16 slice. The times are simulated.
512 devices in a mesh: sp: 16 (over z), dp: 32 (over y, x, core).
Axes of the slice: x: 4, y: 4, z: 16, core: 2. Of those that a mesh axis runs over, the one named last changes fastest.
Arguments:
- tokens: bfloat16 [32, 2048, 2048], P('dp', 'sp'), may hold values from -6 to 6
- receptance_weight: bfloat16 [2048, 1024], P('dp'), may hold values from -0.125 to 0.125
- key_projection_weight: bfloat16 [2048, 1024], P('dp'), may hold values from -0.125 to 0.125
- value_projection_weight: bfloat16 [2048, 1024], P('dp'), may hold values from -0.125 to 0.125
- decay_down_weight: bfloat16 [2048, 256], P('dp'), may hold values from -0.125 to 0.125
- decay_up_weight: bfloat16 [2, 128, 1024], replicated, may hold values from -0.71875 to 0.71875
- decay_floor_level: float32 [2, 1024], replicated, may hold values from -10 to -2.25
- correction_rate_logit: float32 [2, 1024], P(None, 'sp'), may hold values from -4 to 4
- diagonal_address_factor: float32 [2, 1024], P(None, 'sp'), may hold values from -1 to 1
- head_norm_gain: float32 [1024], P('sp'), may hold values from 0.1 to 1.9
Outputs:
- mixed: bfloat16 [32, 2048, 1024], P('dp', 'sp')
All inputs are finite; a program needn't handle non-finite values.
Results may differ from a plain program's by a relative error of at most 0.0056.
The roundings to bfloat16 on the way count: a program that leaves them out, or rounds other values in their place, can miss the bound.
Values may be sent and summed in bfloat16 or wider, within the bound.
No kernel may reach another device: no remote copies, remote signals or barrier semaphores. Data moves between devices by JAX's collectives and lax.ppermute only.
A program may use at most 128 MiB of HBM per device.

v0:
```python
import math
import jax
import jax.numpy as jnp
from jax import lax
from jax.sharding import PartitionSpec as P

SUBSPACE_SIZE = 64


def in_one_piece(arrays, axis, dim, along):
    both = jnp.concatenate(arrays, axis=along)
    result, at, outs = (lax.all_gather(both, axis, axis=dim, tiled=True), 0, [])
    for a in arrays:
        outs.append(lax.slice_in_dim(result, at, at + a.shape[along], axis=along))
        at += a.shape[along]
    return tuple(outs)


def contract(pattern, former, latter):
    return jnp.einsum(pattern, former, latter, precision=lax.Precision.HIGHEST)


def project_rows(totals, pieces, source):
    results = []
    for running, piece in zip(totals, pieces):
        results.append(jnp.dot(source, piece, preferred_element_type=jnp.float32))
    return tuple(results)


def both_ways(content_matrix_full):
    return jnp.stack([content_matrix_full, jnp.flip(content_matrix_full, 0)], 0)


def advance(state, pair):
    transfer_block, inject_block = pair
    later = contract("...ij,...jk->...ik", state, transfer_block) + inject_block
    return (later, state)


def per_device(
    tokens,
    receptance_weight,
    key_projection_weight,
    value_projection_weight,
    decay_down_weight,
    decay_up_weight,
    decay_floor_level,
    correction_rate_logit,
    diagonal_address_factor,
    head_norm_gain,
):
    depth = tokens.shape[2]
    source = tokens.reshape(-1, depth)
    row_count = source.shape[0]
    channels = receptance_weight.shape[1]
    low_width = decay_down_weight.shape[1]
    empty = jnp.zeros((row_count, channels), jnp.float32)
    initial = (empty, empty, empty, jnp.zeros((row_count, low_width), jnp.float32))
    sums = project_rows(
        initial,
        in_one_piece(
            (receptance_weight, key_projection_weight, value_projection_weight, decay_down_weight),
            "dp",
            0,
            1,
        ),
        source,
    )
    receive = sums[0].astype(jnp.bfloat16)
    key_rows = sums[1].astype(jnp.bfloat16)
    value_rows = sums[2].astype(jnp.bfloat16)
    lowered = jnp.tanh(sums[3]).astype(jnp.bfloat16)
    rank = decay_up_weight.shape[1]
    forward_pre = (
        jnp.dot(lowered[:, :rank], decay_up_weight[0], preferred_element_type=jnp.float32)
        + decay_floor_level[0]
    ).astype(jnp.bfloat16)
    backward_pre = (
        jnp.dot(lowered[:, rank:], decay_up_weight[1], preferred_element_type=jnp.float32)
        + decay_floor_level[1]
    ).astype(jnp.bfloat16)
    moved = (
        lax.all_to_all(receive, "sp", split_axis=1, concat_axis=0, tiled=True),
        lax.all_to_all(key_rows, "sp", split_axis=1, concat_axis=0, tiled=True),
        lax.all_to_all(value_rows, "sp", split_axis=1, concat_axis=0, tiled=True),
        lax.all_to_all(forward_pre, "sp", split_axis=1, concat_axis=0, tiled=True),
        lax.all_to_all(backward_pre, "sp", split_axis=1, concat_axis=0, tiled=True),
    )
    length = moved[0].shape[0]
    local_channels = moved[0].shape[1]
    subspace_dimension = SUBSPACE_SIZE
    subspace_batches = local_channels // subspace_dimension
    span = math.gcd(length, 64)
    blocks = length // span

    def by_head(content_matrix_full):
        return content_matrix_full.astype(jnp.float32).reshape(
            length, subspace_batches, subspace_dimension
        )

    def to_blocks(content_matrix_full):
        return jnp.transpose(
            content_matrix_full.reshape(2, blocks, span, subspace_batches, subspace_dimension),
            (0, 3, 1, 2, 4),
        )

    gate_by_subspace = by_head(moved[0])
    address_by_subspace = by_head(moved[1])
    value_per_head = by_head(moved[2])
    amend_strength = jax.nn.sigmoid(correction_rate_logit).reshape(
        2, 1, subspace_batches, subspace_dimension
    )
    normed = address_by_subspace / jnp.sqrt(
        jnp.sum(address_by_subspace * address_by_subspace, -1, keepdims=True) + 1.0
    )
    decay_log = -math.exp(-0.5) * jax.nn.sigmoid(
        jnp.stack([by_head(moved[3]), jnp.flip(by_head(moved[4]), 0)], 0)
    )
    block_rate = jnp.transpose(amend_strength, (0, 2, 1, 3))[:, :, :, None, :]
    probe_matrix_full = to_blocks(both_ways(gate_by_subspace))
    content_matrix_full = to_blocks(both_ways(value_per_head))
    erasers = -to_blocks(both_ways(normed))
    writers = -erasers * block_rate
    rated_keys = to_blocks(both_ways(address_by_subspace)) * block_rate
    log_decay = to_blocks(decay_log)
    inclusive = jnp.cumsum(log_decay, axis=3)
    previous = inclusive - log_decay
    middle = inclusive[:, :, :, span // 2 : span // 2 + 1]
    final = inclusive[:, :, :, span - 1 : span]
    erase_query = erasers * jnp.exp(previous - middle)
    read_query = probe_matrix_full * jnp.exp(inclusive - middle)
    write_key = writers * jnp.exp(middle - inclusive)
    plain_key = rated_keys * jnp.exp(middle - inclusive)
    strict = jnp.tril(jnp.ones((span, span), jnp.bool_), -1)
    lower = jnp.tril(jnp.ones((span, span), jnp.bool_))
    erase_write = jnp.where(strict, contract("...tn,...jn->...tj", erase_query, write_key), 0.0)
    erase_plain = jnp.where(strict, contract("...tn,...jn->...tj", erase_query, plain_key), 0.0)
    read_write = jnp.where(lower, contract("...tn,...jn->...tj", read_query, write_key), 0.0)
    read_plain = jnp.where(lower, contract("...tn,...jn->...tj", read_query, plain_key), 0.0)
    identity = jnp.eye(span, dtype=jnp.float32)
    inverse = lax.linalg.triangular_solve(
        identity - erase_write,
        jnp.broadcast_to(identity, erase_write.shape),
        left_side=True,
        lower=True,
        unit_diagonal=True,
    )
    to_end = jnp.exp(final - inclusive)
    carried = contract("...jt,...jn->...tn", inverse, writers * to_end)
    start_erase = erasers * jnp.exp(previous)
    transfer = contract("...tm,...tn->...mn", start_erase, carried) + jnp.eye(
        subspace_dimension, dtype=jnp.float32
    ) * jnp.exp(final)
    inject = contract(
        "...tv,...tn->...vn",
        content_matrix_full,
        contract("...jt,...jn->...tn", erase_plain, carried) + rated_keys * to_end,
    )
    start_state = jnp.zeros(
        (2, subspace_batches, subspace_dimension, subspace_dimension), jnp.float32
    )
    _, entering = lax.scan(
        advance, start_state, (jnp.moveaxis(transfer, 2, 0), jnp.moveaxis(inject, 2, 0))
    )
    entering = jnp.moveaxis(entering, 0, 2)
    pulled = contract(
        "...tj,...jv->...tv",
        inverse,
        contract("...tk,...vk->...tv", start_erase, entering)
        + contract("...tj,...jv->...tv", erase_plain, content_matrix_full),
    )
    outputs = (
        contract("...tk,...vk->...tv", probe_matrix_full * jnp.exp(inclusive), entering)
        + contract("...tj,...jv->...tv", read_write, pulled)
        + contract("...tj,...jv->...tv", read_plain, content_matrix_full)
    )
    ordered = jnp.transpose(outputs, (0, 2, 3, 1, 4)).reshape(
        2, length, subspace_batches, subspace_dimension
    )
    ordered = jnp.stack([ordered[0], jnp.flip(ordered[1], 0)], 0)
    centred = ordered - jnp.mean(ordered, -1, keepdims=True)
    variance = jnp.mean(centred * centred, -1, keepdims=True)
    gain = head_norm_gain.reshape(1, 1, subspace_batches, subspace_dimension)
    normalized = centred * lax.rsqrt(variance + 0.00064) * gain
    diagonal_extra = diagonal_address_factor.reshape(2, 1, subspace_batches, subspace_dimension)
    diagonal_contribution = (
        jnp.sum(
            gate_by_subspace * address_by_subspace * amend_strength * diagonal_extra,
            -1,
            keepdims=True,
        )
        * value_per_head
    )
    mixed = (
        jnp.sum(normalized + diagonal_contribution, 0)
        .reshape(length, local_channels)
        .astype(jnp.bfloat16)
    )
    returned = lax.all_to_all(mixed, "sp", split_axis=0, concat_axis=1, tiled=True)
    return returned.reshape(1, row_count, channels)


def solution(mesh):
    in_specs = (
        P("dp", "sp", None),
        P("dp", None),
        P("dp", None),
        P("dp", None),
        P("dp", None),
        P(),
        P(),
        P(None, "sp"),
        P(None, "sp"),
        P("sp"),
    )
    out_specs = P("dp", "sp", None)
    return jax.shard_map(
        per_device, mesh=mesh, in_specs=in_specs, out_specs=out_specs, check_vma=False
    )
```

profile of v0, /device:TPU:2, one launch (start us, length us, event | category | flops | bytes accessed | tf_op | source)
XLA Modules:
  0.0 680.4 jit_solution(5575840417447938390)
XLA Ops:
  9.3 86.2 %all-gather.2.cloned.1.call-done = bf16[2048,3328]{1,0:T(8,128)(2,1)} async-done(((bf16[64,3328]{1,0:T(8,128)(2,1)}), bf16[2048,3328]{1,0:T(8,128)(2,1)}) %all-gather.2.cloned.1.call-update) | async-done | bytes 13631504 | tf_op jit(solution)/shard_map/all_gather | solution.py:12
  98.4 12.3 %all-to-all-start.1 = ((bf16[128,16,64]{0,2,1:T(8,128)(2,1)}), bf16[128,16,64]{0,2,1:T(8,128)(2,1)S(1)}, u32[]{:S(2)}, u32[]{:S(2)}) async-start(bf16[128,16,64]{0,2,1:T(8,128)(2,1)} %bitcast.15), calls=%async_computation.1 | async-start | bytes 524288 | tf_op jit(solution)/shard_map/all_to_all | solution.py:86
  110.6 4.2 fusion.63
  114.8 14.4 %all-to-all-done.1 = bf16[128,16,64]{0,2,1:T(8,128)(2,1)S(1)} async-done(((bf16[128,16,64]{0,2,1:T(8,128)(2,1)}), bf16[128,16,64]{0,2,1:T(8,128)(2,1)S(1)}, u32[]{:S(2)}, u32[]{:S(2)}) %all-to-all-start.1) | async-done | bytes 262176 | tf_op jit(solution)/shard_map/all_to_all | solution.py:86
  129.3 6.0 all-to-all-start.4
  135.2 4.2 fusion.60
  139.5 14.1 %all-to-all-done.4 = bf16[128,16,64]{0,2,1:T(8,128)(2,1)S(1)} async-done(((bf16[128,16,64]{0,2,1:T(8,128)(2,1)}), bf16[128,16,64]{0,2,1:T(8,128)(2,1)S(1)}, u32[]{:S(2)}, u32[]{:S(2)}) %all-to-all-start.4) | async-done | bytes 262176 | tf_op jit(solution)/shard_map/all_to_all | solution.py:85
  153.6 5.9 all-to-all-start.3
  159.5 4.2 fusion.57
  163.7 14.3 %all-to-all-done.3 = bf16[128,16,64]{0,2,1:T(8,128)(2,1)S(1)} async-done(((bf16[128,16,64]{0,2,1:T(8,128)(2,1)}), bf16[128,16,64]{0,2,1:T(8,128)(2,1)S(1)}, u32[]{:S(2)}, u32[]{:S(2)}) %all-to-all-start.3) | async-done | bytes 262176 | tf_op jit(solution)/shard_map/all_to_all | solution.py:84
  178.0 5.6 all-to-all-start
  184.9 17.2 %all-to-all-done = bf16[128,16,64]{0,2,1:T(8,128)(2,1)S(1)} async-done(((bf16[128,16,64]{0,2,1:T(8,128)(2,1)}), bf16[128,16,64]{0,2,1:T(8,128)(2,1)S(1)}, u32[]{:S(2)}, u32[]{:S(2)}) %all-to-all-start) | async-done | bytes 262176 | tf_op jit(solution)/shard_map/all_to_all | solution.py:83
  202.1 5.6 all-to-all-start.2
  212.9 5.7 reverse.14
  220.9 5.3 all-to-all-done.2
  227.1 6.7 reverse.13
  239.3 6.7 reverse.12
  254.9 3.2 copy.187
  262.0 7.6 %fusion.87 = f32[2,32,64,64]{3,2,1,0:T(8,128)} fusion(f32[1,32,64,64]{3,2,1,0:T(8,128)S(1)} %bitcast.228, f32[1,32,64,64]{3,2,1,0:T(8,128)S(1)} %bitcast.225, f32[2,1,32,64,64]{4,2,3,1,0:T(8,128)S(1)} %fusion.117, f32[2,32,64]{2,1,0:T(8,128)S(1)} %get-tuple-element.72, f32[1,32,64,64]{3,2,1,0:T(8,128)S(1)} %bitcast.241, ...), kind=kOutput, calls=%fused_computation.119 | convolution fusion | flops 203161600 | bytes 4211200 | tf_op jit(solution)/shard_map/...tn,...jn->...tj/dot_general | solution.py:20
  269.6 7.8 %fusion.89 = f32[2,32,64,64]{3,2,1,0:T(8,128)} fusion(f32[1,32,64,64]{3,2,1,0:T(8,128)S(1)} %bitcast.229, f32[1,32,64,64]{3,2,1,0:T(8,128)S(1)} %bitcast.226, f32[2,1,32,64,64]{4,2,3,1,0:T(8,128)S(1)} %fusion.117, f32[2,32,64]{2,1,0:T(8,128)S(1)} %get-tuple-element.72, f32[2,64]{1,0:T(2,128)S(1)} %add_divide_fusion, f32[1,32,64,64]{3,2,1,0:T(8,128)S(1)} %bitcast.236, ...), kind=kOutput, calls=%fused_computation.120 | convolution fusion | flops 203161600 | bytes 4211200 | tf_op jit(solution)/shard_map/...tn,...jn->...tj/dot_general | solution.py:20
  277.4 8.0 %fusion.85 = f32[2,32,64,64]{3,2,1,0:T(8,128)} fusion(f32[2,32,64]{2,1,0:T(8,128)S(1)} %get-tuple-element.72, f32[1,32,64,64]{3,2,1,0:T(8,128)S(1)} %bitcast.237, f32[1,32,64,64]{3,2,1,0:T(8,128)S(1)} %broadcast_divide_fusion, f32[1,32,64,64]{3,2,1,0:T(8,128)S(1)} %bitcast.242, f32[1,32,64,64]{3,2,1,0:T(8,128)S(1)} %bitcast.233, ...), kind=kOutput, calls=%fused_computation.117 | convolution fusion | flops 204996608 | bytes 5259776 | tf_op jit(solution)/shard_map/...tn,...jn->...tj/dot_general | solution.py:20
  285.4 8.3 %fusion.86 = f32[2,32,64,64]{3,2,1,0:T(8,128)} fusion(f32[2,32,64]{2,1,0:T(8,128)S(1)} %get-tuple-element.72, f32[1,32,64,64]{3,2,1,0:T(8,128)S(1)} %bitcast.238, f32[1,32,64,64]{3,2,1,0:T(8,128)S(1)} %broadcast_divide_fusion, f32[2,1,32,64,64]{4,2,3,1,0:T(8,128)S(1)} %fusion.117, f32[2,64]{1,0:T(2,128)S(1)} %add_divide_fusion, ...), kind=kOutput, calls=%fused_computation.118 | convolution fusion | flops 204996608 | bytes 4211200 | tf_op jit(solution)/shard_map/...tn,...jn->...tj/dot_general | solution.py:20
  304.3 3.8 copy.210
  308.1 3.9 copy.215
  312.0 3.9 copy.196
  315.8 7.9 %broadcast_select_fusion.1 = (f32[2,32,64,64]{1,3,2,0:T(8,128)}, f32[2,1,32,1,64,64]{2,5,4,3,1,0:T(8,128)}) fusion(f32[2,32,64,64]{1,3,2,0:T(8,128)} %copy.210, pred[64,64]{1,0:T(8,128)(4,1)S(1)} %get-tuple-element.87, f32[64,64]{1,0:T(8,128)S(1)} %fusion.96, f32[2,32,64,64]{1,3,2,0:T(8,128)} %copy.196, f32[64,64]{1,0:T(8,128)S(1)} %get-tuple-element.88), kind=kLoop, calls=%fused_computation.54 | loop fusion | flops 1310720 | bytes 4231168 | tf_op jit(solution)/shard_map/jit(_where)/select_n | solution.py:137
  323.7 4.1 copy.217
  327.8 3.8 copy.220
  331.7 6.4 broadcast_select_fusion
  338.1 4.1 copy.219
  342.2 4.1 copy.221
  346.3 134.0 %custom-call.3 = f32[2,1,32,1,64,64]{2,4,5,3,1,0:T(8,128)} custom-call(f32[2,1,32,1,64,64]{2,5,4,3,1,0:T(8,128)} %get-tuple-element.80), custom_call_target="InvertDiagBlocksLowerTriangular" | custom-call | tf_op jit(solution)/shard_map/triangular_solve | solution.py:141
  480.3 5.4 copy.197
  485.8 3.7 fusion.69
  490.8 4.9 fusion.33
  495.7 6.5 fusion.80
  502.2 4.0 fusion.118
  506.3 4.8 fusion.51
  511.1 4.8 fusion.50
  516.0 5.2 fusion.42
  521.1 3.9 copy.202
  525.0 4.0 add_bitcast_fusion
  529.1 5.3 copy.212
  534.3 84.6 %while.12 = (s32[]{:T(128)}, f32[2,1,64,64]{2,3,0,1:T(8,128)S(1)}, f32[32,2,1,64,64]{3,4,1,2,0:T(8,128)}, f32[32,2,1,64,64]{3,4,1,2,0:T(8,128)}, f32[32,2,1,64,64]{4,3,0,1,2:T(8,128)}, /*index=5*/s32[]{:T(128)}) while((s32[]{:T(128)}, f32[2,1,64,64]{2,3,0,1:T(8,128)S(1)}, f32[32,2,1,64,64]{3,4,1,2,0:T(8,128)}, ...), condition=%wide.region_3.4_spmd, body=%wide.region_2.3_spmd.sunk | while | flops 6299650 | bytes 458841 | solution.py:162
  619.0 6.8 %fusion.35 = f32[2,32,64,64]{3,2,1,0:T(8,128)S(1)} fusion(f32[1,32,64,64]{3,2,1,0:T(8,128)} %bitcast.235, f32[1,32,64,64]{3,2,1,0:T(8,128)} %copy-done.15, f32[1,32,64,64]{3,2,1,0:T(8,128)} %bitcast.254, f32[1,32,64,64]{3,2,1,0:T(8,128)} %bitcast.250, f32[2,1,32,64,64]{4,2,3,1,0:T(8,128)S(1)} %fusion.117, f32[32,2,1,64,64]{3,4,1,2,0:T(8,128)} %get-tuple-element.32), kind=kOutput, calls=%fused_computation.58 | convolution fusion | flops 203685888 | bytes 5242880 | tf_op jit(solution)/shard_map/...tk,...vk->...tv/dot_general | solution.py:20
  631.0 4.2 add_add_fusion
  636.4 6.8 %rev.12 = f32[2048,1,64]{2,0,1:T(8,128)S(1)} reverse(f32[2048,1,64]{2,0,1:T(8,128)} %bitcast.247), dimensions={0} | reverse | bytes 1048576 | tf_op jit(solution)/shard_map/jit(_flip)/rev | solution.py:180
  647.8 24.7 %all_to_all.78 = bf16[16,128,64]{1,2,0:T(8,128)(2,1)S(1)} all-to-all(bf16[16,128,64]{1,2,0:T(8,128)(2,1)S(1)} %copy_bitcast_fusion.4), channel_id=1, replica_groups=mesh['sp'=16,'dp'=32] {'sp'}, dimensions={0} | all-to-all | bytes 524288 | tf_op jit(solution)/shard_map/all_to_all | solution.py:199
  (298 shorter events, 140.3 us)
Async XLA Ops:
  6.5 89.0 %copy-start = (bf16[1,128,2048]{2,1,0:T(8,128)(2,1)S(1)}, bf16[1,128,2048]{2,1,0:T(8,128)(2,1)}, u32[]{:S(2)}) copy-start(bf16[1,128,2048]{2,1,0:T(8,128)(2,1)} %param.12) | copy-start | bytes 1572868
  6.5 90.7 %copy-start.32 = (bf16[2,128,1024]{2,1,0:T(8,128)(2,1)S(1)}, bf16[2,128,1024]{2,1,0:T(8,128)(2,1)}, u32[]{:S(2)}) copy-start(bf16[2,128,1024]{2,1,0:T(8,128)(2,1)} %param.17) | copy-start | bytes 1572868
  6.5 89.0 %all-gather.2.cloned.1.call-start = ((), (), s32[]{:S(2)}) async-start(), calls=%async_computation.6 | async-start | bytes 14057472 | tf_op jit(solution)/shard_map/all_gather | solution.py:12
  98.4 30.9 %all-to-all-start.1 = ((bf16[128,16,64]{0,2,1:T(8,128)(2,1)}), bf16[128,16,64]{0,2,1:T(8,128)(2,1)S(1)}, u32[]{:S(2)}, u32[]{:S(2)}) async-start(bf16[128,16,64]{0,2,1:T(8,128)(2,1)} %bitcast.15), calls=%async_computation.1 | async-start | bytes 524288 | tf_op jit(solution)/shard_map/all_to_all | solution.py:86
  129.3 24.3 %all-to-all-start.4 = ((bf16[128,16,64]{0,2,1:T(8,128)(2,1)}), bf16[128,16,64]{0,2,1:T(8,128)(2,1)S(1)}, u32[]{:S(2)}, u32[]{:S(2)}) async-start(bf16[128,16,64]{0,2,1:T(8,128)(2,1)} %bitcast.38), calls=%async_computation.4 | async-start | bytes 524288 | tf_op jit(solution)/shard_map/all_to_all | solution.py:85
  153.6 24.5 %all-to-all-start.3 = ((bf16[128,16,64]{0,2,1:T(8,128)(2,1)}), bf16[128,16,64]{0,2,1:T(8,128)(2,1)S(1)}, u32[]{:S(2)}, u32[]{:S(2)}) async-start(bf16[128,16,64]{0,2,1:T(8,128)(2,1)} %bitcast.23), calls=%async_computation.3 | async-start | bytes 524288 | tf_op jit(solution)/shard_map/all_to_all | solution.py:84
  159.5 24.1 %copy-start.34 = (f32[2,64]{1,0:T(2,128)S(1)}, f32[2,64]{1,0:T(2,128)}, u32[]{:S(2)}) copy-start(f32[2,64]{1,0:T(2,128)} %param.19) | copy-start | bytes 1540
  178.0 24.1 %all-to-all-start = ((bf16[128,16,64]{0,2,1:T(8,128)(2,1)}), bf16[128,16,64]{0,2,1:T(8,128)(2,1)S(1)}, u32[]{:S(2)}, u32[]{:S(2)}) async-start(bf16[128,16,64]{0,2,1:T(8,128)(2,1)} %bitcast.8), calls=%async_computation | async-start | bytes 524288 | tf_op jit(solution)/shard_map/all_to_all | solution.py:83
  202.1 24.1 %all-to-all-start.2 = ((bf16[128,16,64]{0,2,1:T(8,128)(2,1)}), bf16[128,16,64]{0,2,1:T(8,128)(2,1)S(1)}, u32[]{:S(2)}, u32[]{:S(2)}) async-start(bf16[128,16,64]{0,2,1:T(8,128)(2,1)} %bitcast.19), calls=%async_computation.2 | async-start | bytes 524288 | tf_op jit(solution)/shard_map/all_to_all | solution.py:87
  246.0 3.9 copy-start.26
  258.1 2.0 copy-start.11
  258.1 2.3 copy-start.17
  260.0 1.3 copy-start.5
  260.0 2.0 copy-start.7
  260.4 25.0 %copy-start.15 = (f32[1,32,64,64]{3,2,1,0:T(8,128)}, f32[1,32,64,64]{3,2,1,0:T(8,128)S(1)}, u32[]{:S(2)}) copy-start(f32[1,32,64,64]{3,2,1,0:T(8,128)S(1)} %broadcast_divide_fusion) | copy-start | bytes 1572868
  262.0 7.6 %copy-start.13 = (f32[2048,1,64]{2,0,1:T(8,128)S(1)}, f32[2048,1,64]{2,0,1:T(8,128)}, u32[]{:S(2)}) copy-start(f32[2048,1,64]{2,0,1:T(8,128)} %copy.236) | copy-start | bytes 1572868
  269.6 7.8 %copy-start.28 = (f32[16,128,64]{2,1,0:T(8,128)S(1)}, f32[16,128,64]{2,1,0:T(8,128)}, u32[]{:S(2)}) copy-start(f32[16,128,64]{2,1,0:T(8,128)} %copy.237) | copy-start | bytes 1572868
  269.6 7.8 %copy-start.30 = (f32[2048,64]{1,0:T(8,128)S(1)}, f32[2048,64]{1,0:T(8,128)}, u32[]{:S(2)}) copy-start(f32[2048,64]{1,0:T(8,128)} %copy.238) | copy-start | bytes 1572868
  285.4 8.3 %copy-start.25 = (f32[16,128,64]{1,2,0:T(8,128)S(1)}, f32[16,128,64]{1,2,0:T(8,128)}, u32[]{:S(2)}) copy-start(f32[16,128,64]{1,2,0:T(8,128)} %get-tuple-element.73) | copy-start | bytes 1572868
  294.8 5.1 copy-start.24
  485.7 5.0 copy-start.14
  485.7 5.0 copy-start.16
  489.4 1.3 copy-start.3
  490.8 4.9 copy-start.29
  490.8 4.9 copy-start.31
  495.7 6.5 copy-start.2
  502.2 4.0 copy-start.9
  502.2 4.0 copy-start.10
  506.3 4.8 copy-start.20
  511.1 4.8 copy-start.12
  511.1 4.8 copy-start.18
  618.9 6.8 %copy-start.4 = (f32[2,32,64,64]{3,2,1,0:T(8,128)S(1)}, f32[2,32,64,64]{3,2,1,0:T(8,128)}, u32[]{:S(2)}) copy-start(f32[2,32,64,64]{3,2,1,0:T(8,128)} %copy-done.3) | copy-start | bytes 3145732
  618.9 6.8 %copy-start.22 = (f32[2,32,64,64]{3,2,1,0:T(8,128)S(1)}, f32[2,32,64,64]{3,2,1,0:T(8,128)}, u32[]{:S(2)}) copy-start(f32[2,32,64,64]{3,2,1,0:T(8,128)} %fusion.51) | copy-start | bytes 3145732
  625.8 2.3 copy-start.19
  628.1 2.4 copy-start.6
  628.1 2.4 copy-start.8
  628.1 2.4 copy-start.21
  628.1 2.8 copy-start.27
  643.2 2.0 copy-start.33
  643.2 2.2 copy-start.23
  643.2 2.2 copy-start.35
  645.4 27.9 %copy-start.1 = (bf16[1,128,2048]{2,1,0:T(8,128)(2,1)S(1)}, bf16[1,128,2048]{2,1,0:T(8,128)(2,1)}, u32[]{:S(2)}) copy-start(bf16[1,128,2048]{2,1,0:T(8,128)(2,1)} %param.12) | copy-start | bytes 1572868
Sparse Core Ops, SparseCore 0:
  10.5 85.0 all-gather.1
where the time goes:
time: 694 us; the launch traced here: 680 us
  other arithmetic  165 us (24%)
  local copies, waits for them, and re-layouts  159 us (23%)
  waiting for transfers between devices  152 us (22%)
  matrix products  129 us (19%)
  starting transfers between devices  35.3 us (5%)
  blocking collectives  24.7 us (4%)
  between operations  14.3 us (2%)
    another operation x4, other arithmetic, per_device(): lax.linalg.triangular_solve(identity - erase_write, jnp.broadcast_to(iden...  134 us
    dot_general x46, matrix products, contract(): return jnp.einsum(pattern, former, latter, precision=lax.Precision.HIGHEST)  110 us
    all_gather x1, waiting for transfers between devices, in_one_piece(): result, at, outs = (lax.all_gather(both, axis, axis=dim, tiled=True), 0, [])  86.2 us
    dynamic_slice x64, local copies, waits for them, and re-layouts, per_device(): lax.scan(advance, start_state, (jnp.moveaxis(transfer, 2, 0), jnp.moveaxi...  29.9 us
    another operation x5, local copies, waits for them, and re-layouts  25.8 us
    all_to_all x1, blocking collectives, per_device(): lax.all_to_all(mixed, 'sp', split_axis=0, concat_axis=1, tiled=True)  24.7 us
    dynamic_update_slice x32, local copies, waits for them, and re-layouts, per_device(): lax.scan(advance, start_state, (jnp.moveaxis(transfer, 2, 0), jnp.moveaxi...  20.4 us
    dot_general x5, local copies, waits for them, and re-layouts, contract(): return jnp.einsum(pattern, former, latter, precision=lax.Precision.HIGHEST)  19.3 us
  transfers between devices with their start and end apart: 6, of which 6 were waited for; matrix products, arithmetic and copies ran while one was open for 4% of the time, Pallas kernels for 0%

commit v1 on v0

--- a/solution.py
+++ b/solution.py
@@ -82,7 +82,12 @@
     moved = (
         lax.all_to_all(receive, "sp", split_axis=1, concat_axis=0, tiled=True),
         lax.all_to_all(key_rows, "sp", split_axis=1, concat_axis=0, tiled=True),
-        lax.all_to_all(value_rows, "sp", split_axis=1, concat_axis=0, tiled=True),
+        jnp.concatenate(
+            lax.all_to_all(
+                jnp.stack(jnp.split(value_rows, lax.axis_size("sp"), axis=1)), "sp", 0, 0
+            ),
+            axis=0,
+        ),
         lax.all_to_all(forward_pre, "sp", split_axis=1, concat_axis=0, tiled=True),
         lax.all_to_all(backward_pre, "sp", split_axis=1, concat_axis=0, tiled=True),
     )

time: 694 us -> 695 us (level)
  waiting for transfers between devices: 152 us -> 142 us
  local copies, waits for them, and re-layouts: 159 us -> 168 us
    unnamed x72 -> x93, local copies, waits for them, and re-layouts: 3.51 us -> 12.5 us
    all_to_all x1, waiting for transfers between devices: 14.4 us -> 5.52 us  [per_device(): lax.all_to_all(forward_pre, 'sp', split_axis=1, concat_axis=0, tiled=True)]
    another operation x5 -> x6, local copies, waits for them, and re-layouts: 25.8 us -> 26.4 us
    convert_element_type x13 -> x12, local copies, waits for them, and re-layouts: 14 us -> 13.7 us  [by_head(): content_matrix_full.astype(jnp.float32)]
  transfers between devices with their start and end apart: 6 -> 6, of which waited for: 6 -> 6; matrix products, arithmetic and copies ran while one was open for 4% -> 5% of each run, Pallas kernels for 0% -> 0%
where the time goes in v1:
time: 695 us; the launch traced here: 681 us
  local copies, waits for them, and re-layouts  168 us (24%)
  other arithmetic  167 us (24%)
  waiting for transfers between devices  142 us (20%)
  matrix products  128 us (18%)
  starting transfers between devices  35.5 us (5%)
  blocking collectives  23.9 us (3%)
  between operations  14.3 us (2%)
    another operation x4, other arithmetic, per_device(): lax.linalg.triangular_solve(identity - erase_write, jnp.broadcast_to(iden...  135 us
    dot_general x46, matrix products, contract(): return jnp.einsum(pattern, former, latter, precision=lax.Precision.HIGHEST)  111 us
    all_gather x1, waiting for transfers between devices, in_one_piece(): result, at, outs = (lax.all_gather(both, axis, axis=dim, tiled=True), 0, [])  86.2 us
    dynamic_slice x64, local copies, waits for them, and re-layouts, per_device(): lax.scan(advance, start_state, (jnp.moveaxis(transfer, 2, 0), jnp.moveaxi...  29.9 us
    another operation x5, local copies, waits for them, and re-layouts  25.8 us
    all_to_all x1, blocking collectives, per_device(): lax.all_to_all(mixed, 'sp', split_axis=0, concat_axis=1, tiled=True)  23.9 us
    dynamic_update_slice x32, local copies, waits for them, and re-layouts, per_device(): lax.scan(advance, start_state, (jnp.moveaxis(transfer, 2, 0), jnp.moveaxi...  20.3 us
    dot_general x5, local copies, waits for them, and re-layouts, contract(): return jnp.einsum(pattern, former, latter, precision=lax.Precision.HIGHEST)  19.3 us
  transfers between devices with their start and end apart: 6, of which 6 were waited for; matrix products, arithmetic and copies ran while one was open for 5% of the time, Pallas kernels for 0%

profile of v1, /device:TPU:2, one launch (start us, length us, event | category | flops | bytes accessed | tf_op | source)
XLA Modules:
  0.0 680.8 jit_solution(223557860400539103)
XLA Ops:
  9.3 86.2 %all-gather.2.cloned.1.call-done = bf16[2048,3328]{1,0:T(8,128)(2,1)} async-done(((bf16[64,3328]{1,0:T(8,128)(2,1)}), bf16[2048,3328]{1,0:T(8,128)(2,1)}) %all-gather.2.cloned.1.call-update) | async-done | bytes 13631504 | tf_op jit(solution)/shard_map/all_gather | solution.py:12
  98.4 12.3 %all-to-all-start.1 = ((bf16[128,16,64]{0,2,1:T(8,128)(2,1)}), bf16[128,16,64]{0,2,1:T(8,128)(2,1)S(1)}, u32[]{:S(2)}, u32[]{:S(2)}) async-start(bf16[128,16,64]{0,2,1:T(8,128)(2,1)} %bitcast.15), calls=%async_computation.1 | async-start | bytes 524288 | tf_op jit(solution)/shard_map/all_to_all | solution.py:91
  110.6 3.5 fusion.66
  123.7 5.5 all-to-all-done.1
  129.3 6.5 all-to-all-start.4
  135.8 4.2 fusion.60
  140.0 14.2 %all-to-all-done.4 = bf16[16,128,64]{1,2,0:T(8,128)(2,1)S(1)} async-done(((bf16[16,128,64]{1,2,0:T(8,128)(2,1)}), bf16[16,128,64]{1,2,0:T(8,128)(2,1)S(1)}, u32[]{:S(2)}, u32[]{:S(2)}) %all-to-all-start.4) | async-done | bytes 262176 | tf_op jit(solution)/shard_map/all_to_all | solution.py:86
  154.2 5.6 all-to-all-start.3
  161.0 4.2 fusion.57
  165.2 13.1 %all-to-all-done.3 = bf16[128,16,64]{0,2,1:T(8,128)(2,1)S(1)} async-done(((bf16[128,16,64]{0,2,1:T(8,128)(2,1)}), bf16[128,16,64]{0,2,1:T(8,128)(2,1)S(1)}, u32[]{:S(2)}, u32[]{:S(2)}) %all-to-all-start.3) | async-done | bytes 262176 | tf_op jit(solution)/shard_map/all_to_all | solution.py:84
  178.3 5.6 all-to-all-start
  185.7 16.7 %all-to-all-done = bf16[128,16,64]{0,2,1:T(8,128)(2,1)S(1)} async-done(((bf16[128,16,64]{0,2,1:T(8,128)(2,1)}), bf16[128,16,64]{0,2,1:T(8,128)(2,1)S(1)}, u32[]{:S(2)}, u32[]{:S(2)}) %all-to-all-start) | async-done | bytes 262176 | tf_op jit(solution)/shard_map/all_to_all | solution.py:83
  202.4 5.6 all-to-all-start.2
  208.1 5.6 reverse.14
  220.2 6.4 all-to-all-done.2
  228.4 6.7 reverse.13
  240.6 6.7 reverse.12
  256.2 3.2 copy.188
  263.3 7.6 %fusion.90 = f32[2,32,64,64]{3,2,1,0:T(8,128)} fusion(f32[1,32,64,64]{3,2,1,0:T(8,128)S(1)} %bitcast.289, f32[1,32,64,64]{3,2,1,0:T(8,128)S(1)} %bitcast.286, f32[2,1,32,64,64]{4,2,3,1,0:T(8,128)S(1)} %fusion.120, f32[2,32,64]{2,1,0:T(8,128)S(1)} %get-tuple-element.72, f32[1,32,64,64]{3,2,1,0:T(8,128)S(1)} %bitcast.302, ...), kind=kOutput, calls=%fused_computation.118 | convolution fusion | flops 203161600 | bytes 4211200 | tf_op jit(solution)/shard_map/...tn,...jn->...tj/dot_general | solution.py:20
  271.0 7.8 %fusion.92 = f32[2,32,64,64]{3,2,1,0:T(8,128)} fusion(f32[1,32,64,64]{3,2,1,0:T(8,128)S(1)} %bitcast.290, f32[1,32,64,64]{3,2,1,0:T(8,128)S(1)} %bitcast.287, f32[2,1,32,64,64]{4,2,3,1,0:T(8,128)S(1)} %fusion.120, f32[2,32,64]{2,1,0:T(8,128)S(1)} %get-tuple-element.72, f32[2,64]{1,0:T(2,128)S(1)} %copy-done.32, f32[1,32,64,64]{3,2,1,0:T(8,128)S(1)} %bitcast.297, ...), kind=kOutput, calls=%fused_computation.119 | convolution fusion | flops 203161600 | bytes 4211200 | tf_op jit(solution)/shard_map/...tn,...jn->...tj/dot_general | solution.py:20
  278.8 8.0 %fusion.88 = f32[2,32,64,64]{3,2,1,0:T(8,128)} fusion(f32[2,32,64]{2,1,0:T(8,128)S(1)} %get-tuple-element.72, f32[1,32,64,64]{3,2,1,0:T(8,128)S(1)} %bitcast.298, f32[1,32,64,64]{3,2,1,0:T(8,128)S(1)} %broadcast_divide_fusion, f32[1,32,64,64]{3,2,1,0:T(8,128)S(1)} %bitcast.303, f32[1,32,64,64]{3,2,1,0:T(8,128)S(1)} %bitcast.294, ...), kind=kOutput, calls=%fused_computation.116 | convolution fusion | flops 204996608 | bytes 5259776 | tf_op jit(solution)/shard_map/...tn,...jn->...tj/dot_general | solution.py:20
  286.8 8.3 %fusion.89 = f32[2,32,64,64]{3,2,1,0:T(8,128)} fusion(f32[2,32,64]{2,1,0:T(8,128)S(1)} %get-tuple-element.72, f32[1,32,64,64]{3,2,1,0:T(8,128)S(1)} %bitcast.299, f32[1,32,64,64]{3,2,1,0:T(8,128)S(1)} %broadcast_divide_fusion, f32[2,1,32,64,64]{4,2,3,1,0:T(8,128)S(1)} %fusion.120, f32[2,64]{1,0:T(2,128)S(1)} %copy-done.32, ...), kind=kOutput, calls=%fused_computation.117 | convolution fusion | flops 204996608 | bytes 4211200 | tf_op jit(solution)/shard_map/...tn,...jn->...tj/dot_general | solution.py:20
  305.5 3.8 copy.211
  309.3 3.9 copy.216
  313.1 3.9 copy.197
  317.0 7.8 %broadcast_select_fusion.1 = (f32[2,32,64,64]{1,3,2,0:T(8,128)}, f32[2,1,32,1,64,64]{2,5,4,3,1,0:T(8,128)}) fusion(f32[2,32,64,64]{1,3,2,0:T(8,128)} %copy.211, pred[64,64]{1,0:T(8,128)(4,1)S(1)} %copy-done.35, f32[64,64]{1,0:T(8,128)S(1)} %fusion.99, f32[2,32,64,64]{1,3,2,0:T(8,128)} %copy.197, f32[64,64]{1,0:T(8,128)S(1)} %get-tuple-element.86), kind=kLoop, calls=%fused_computation.54 | loop fusion | flops 1310720 | bytes 4231168 | tf_op jit(solution)/shard_map/jit(_where)/select_n | solution.py:142
  324.9 4.1 copy.218
  329.0 3.8 copy.221
  332.8 6.4 broadcast_select_fusion
  339.2 4.1 copy.220
  343.3 4.1 copy.222
  347.4 134.0 %custom-call.3 = f32[2,1,32,1,64,64]{2,4,5,3,1,0:T(8,128)} custom-call(f32[2,1,32,1,64,64]{2,5,4,3,1,0:T(8,128)} %get-tuple-element.78), custom_call_target="InvertDiagBlocksLowerTriangular" | custom-call | tf_op jit(solution)/shard_map/triangular_solve | solution.py:146
  481.5 5.4 copy.198
  486.9 3.7 fusion.72
  491.9 4.9 fusion.33
  496.9 6.5 fusion.83
  503.4 4.0 fusion.121
  507.5 4.8 fusion.51
  512.3 4.8 fusion.50
  517.1 5.2 fusion.42
  522.3 3.9 copy.203
  526.2 4.0 add_bitcast_fusion
  530.3 5.3 copy.213
  535.5 84.6 %while.12 = (s32[]{:T(128)}, f32[2,1,64,64]{2,3,0,1:T(8,128)S(1)}, f32[32,2,1,64,64]{3,4,1,2,0:T(8,128)}, f32[32,2,1,64,64]{3,4,1,2,0:T(8,128)}, f32[32,2,1,64,64]{4,3,0,1,2:T(8,128)}, /*index=5*/s32[]{:T(128)}) while((s32[]{:T(128)}, f32[2,1,64,64]{2,3,0,1:T(8,128)S(1)}, f32[32,2,1,64,64]{3,4,1,2,0:T(8,128)}, ...), condition=%wide.region_3.4_spmd, body=%wide.region_2.3_spmd.sunk | while | flops 6299650 | bytes 458841 | solution.py:167
  620.2 6.8 %fusion.35 = f32[2,32,64,64]{3,2,1,0:T(8,128)S(1)} fusion(f32[1,32,64,64]{3,2,1,0:T(8,128)} %bitcast.296, f32[1,32,64,64]{3,2,1,0:T(8,128)} %copy-done.15, f32[1,32,64,64]{3,2,1,0:T(8,128)} %bitcast.313, f32[1,32,64,64]{3,2,1,0:T(8,128)} %bitcast.309, f32[2,1,32,64,64]{4,2,3,1,0:T(8,128)S(1)} %fusion.120, f32[32,2,1,64,64]{3,4,1,2,0:T(8,128)} %get-tuple-element.32), kind=kOutput, calls=%fused_computation.58 | convolution fusion | flops 203685888 | bytes 5242880 | tf_op jit(solution)/shard_map/...tk,...vk->...tv/dot_general | solution.py:20
  632.2 4.2 add_add_fusion
  637.6 6.8 %rev.12 = f32[2048,1,64]{2,0,1:T(8,128)S(1)} reverse(f32[2048,1,64]{2,0,1:T(8,128)} %bitcast.306), dimensions={0} | reverse | bytes 1048576 | tf_op jit(solution)/shard_map/jit(_flip)/rev | solution.py:185
  649.0 23.9 %all_to_all.70 = bf16[16,128,64]{1,2,0:T(8,128)(2,1)S(1)} all-to-all(bf16[16,128,64]{1,2,0:T(8,128)(2,1)S(1)} %copy_bitcast_fusion.4), channel_id=1, replica_groups=mesh['sp'=16,'dp'=32] {'sp'}, dimensions={0} | all-to-all | bytes 524288 | tf_op jit(solution)/shard_map/all_to_all | solution.py:204
  (319 shorter events, 151.3 us)
Async XLA Ops:
  6.5 89.0 %copy-start = (bf16[1,128,2048]{2,1,0:T(8,128)(2,1)S(1)}, bf16[1,128,2048]{2,1,0:T(8,128)(2,1)}, u32[]{:S(2)}) copy-start(bf16[1,128,2048]{2,1,0:T(8,128)(2,1)} %param.12) | copy-start | bytes 1572868
  6.5 90.7 %copy-start.31 = (bf16[2,128,1024]{2,1,0:T(8,128)(2,1)S(1)}, bf16[2,128,1024]{2,1,0:T(8,128)(2,1)}, u32[]{:S(2)}) copy-start(bf16[2,128,1024]{2,1,0:T(8,128)(2,1)} %param.17) | copy-start | bytes 1572868
  6.5 89.0 %all-gather.2.cloned.1.call-start = ((), (), s32[]{:S(2)}) async-start(), calls=%async_computation.6 | async-start | bytes 14057472 | tf_op jit(solution)/shard_map/all_gather | solution.py:12
  98.4 30.9 %all-to-all-start.1 = ((bf16[128,16,64]{0,2,1:T(8,128)(2,1)}), bf16[128,16,64]{0,2,1:T(8,128)(2,1)S(1)}, u32[]{:S(2)}, u32[]{:S(2)}) async-start(bf16[128,16,64]{0,2,1:T(8,128)(2,1)} %bitcast.15), calls=%async_computation.1 | async-start | bytes 524288 | tf_op jit(solution)/shard_map/all_to_all | solution.py:91
  129.3 25.0 %all-to-all-start.4 = ((bf16[16,128,64]{1,2,0:T(8,128)(2,1)}), bf16[16,128,64]{1,2,0:T(8,128)(2,1)S(1)}, u32[]{:S(2)}, u32[]{:S(2)}) async-start(bf16[16,128,64]{1,2,0:T(8,128)(2,1)} %constant_dynamic-update-slice_fusion), calls=%async_computation.4 | async-start | bytes 524288 | tf_op jit(solution)/shard_map/all_to_all | solution.py:86
  135.8 24.6 %copy-start.37 = (f32[2,64]{1,0:T(2,128)S(1)}, f32[2,64]{1,0:T(2,128)}, u32[]{:S(2)}) copy-start(f32[2,64]{1,0:T(2,128)} %param.19) | copy-start | bytes 1540
  154.2 24.1 %all-to-all-start.3 = ((bf16[128,16,64]{0,2,1:T(8,128)(2,1)}), bf16[128,16,64]{0,2,1:T(8,128)(2,1)S(1)}, u32[]{:S(2)}, u32[]{:S(2)}) async-start(bf16[128,16,64]{0,2,1:T(8,128)(2,1)} %bitcast.23), calls=%async_computation.3 | async-start | bytes 524288 | tf_op jit(solution)/shard_map/all_to_all | solution.py:84
  178.3 24.1 %all-to-all-start = ((bf16[128,16,64]{0,2,1:T(8,128)(2,1)}), bf16[128,16,64]{0,2,1:T(8,128)(2,1)S(1)}, u32[]{:S(2)}, u32[]{:S(2)}) async-start(bf16[128,16,64]{0,2,1:T(8,128)(2,1)} %bitcast.8), calls=%async_computation | async-start | bytes 524288 | tf_op jit(solution)/shard_map/all_to_all | solution.py:83
  202.4 24.2 %all-to-all-start.2 = ((bf16[128,16,64]{0,2,1:T(8,128)(2,1)}), bf16[128,16,64]{0,2,1:T(8,128)(2,1)}, u32[]{:S(2)}, u32[]{:S(2)}) async-start(bf16[128,16,64]{0,2,1:T(8,128)(2,1)} %bitcast.19), calls=%async_computation.2 | async-start | bytes 524288 | tf_op jit(solution)/shard_map/all_to_all | solution.py:92
  239.3 9.4 %copy-start.25 = (f32[16,8,8,128]{3,2,0,1:T(8,128)S(1)}, f32[16,8,8,128]{3,2,0,1:T(8,128)}, u32[]{:S(2)}) copy-start(f32[16,8,8,128]{3,2,0,1:T(8,128)} %copy.303) | copy-start | bytes 1572868
  259.4 2.0 copy-start.11
  259.4 2.3 copy-start.17
  261.3 1.3 copy-start.5
  261.4 2.0 copy-start.7
  261.4 2.0 copy-start.32
  261.8 25.0 %copy-start.15 = (f32[1,32,64,64]{3,2,1,0:T(8,128)}, f32[1,32,64,64]{3,2,1,0:T(8,128)S(1)}, u32[]{:S(2)}) copy-start(f32[1,32,64,64]{3,2,1,0:T(8,128)S(1)} %broadcast_divide_fusion) | copy-start | bytes 1572868
  263.3 7.6 %copy-start.13 = (f32[2048,1,64]{2,0,1:T(8,128)S(1)}, f32[2048,1,64]{2,0,1:T(8,128)}, u32[]{:S(2)}) copy-start(f32[2048,1,64]{2,0,1:T(8,128)} %copy.237) | copy-start | bytes 1572868
  271.0 7.8 %copy-start.27 = (f32[16,128,64]{2,1,0:T(8,128)S(1)}, f32[16,128,64]{2,1,0:T(8,128)}, u32[]{:S(2)}) copy-start(f32[16,128,64]{2,1,0:T(8,128)} %copy.238) | copy-start | bytes 1572868
  271.0 7.8 %copy-start.29 = (f32[2048,64]{1,0:T(8,128)S(1)}, f32[2048,64]{1,0:T(8,128)}, u32[]{:S(2)}) copy-start(f32[2048,64]{1,0:T(8,128)} %copy.239) | copy-start | bytes 1572868
  295.1 6.0 copy-start.24
  313.1 3.9 copy-start.35
  329.0 3.8 copy-start.34
  486.9 5.0 copy-start.14
  486.9 5.0 copy-start.16
  486.9 5.0 copy-start.33
  490.6 1.3 copy-start.3
  491.9 4.9 copy-start.28
  491.9 4.9 copy-start.30
  496.9 6.5 copy-start.2
  503.4 4.0 copy-start.9
  503.4 4.0 copy-start.10
  507.4 4.8 copy-start.20
  512.3 4.8 copy-start.12
  512.3 4.8 copy-start.18
  620.1 6.8 %copy-start.4 = (f32[2,32,64,64]{3,2,1,0:T(8,128)S(1)}, f32[2,32,64,64]{3,2,1,0:T(8,128)}, u32[]{:S(2)}) copy-start(f32[2,32,64,64]{3,2,1,0:T(8,128)} %copy-done.3) | copy-start | bytes 3145732
  620.1 6.8 %copy-start.22 = (f32[2,32,64,64]{3,2,1,0:T(8,128)S(1)}, f32[2,32,64,64]{3,2,1,0:T(8,128)}, u32[]{:S(2)}) copy-start(f32[2,32,64,64]{3,2,1,0:T(8,128)} %fusion.51) | copy-start | bytes 3145732
  627.0 2.3 copy-start.19
  629.3 2.4 copy-start.6
  629.3 2.4 copy-start.8
  629.3 2.4 copy-start.21
  629.3 2.8 copy-start.26
  644.4 2.0 copy-start.36
  644.4 2.2 copy-start.23
  644.4 2.2 copy-start.38
  646.6 27.1 %copy-start.1 = (bf16[1,128,2048]{2,1,0:T(8,128)(2,1)S(1)}, bf16[1,128,2048]{2,1,0:T(8,128)(2,1)}, u32[]{:S(2)}) copy-start(bf16[1,128,2048]{2,1,0:T(8,128)(2,1)} %param.12) | copy-start | bytes 1572868
Sparse Core Ops, SparseCore 0:
  10.5 85.0 all-gather.1
